TPU v7x, 32 devices: a whole 2x2x4 slice. The times are simulated.
32 devices in a mesh: ep: 8 (over z, y), tp: 4 (over x, core).
Axes of the slice: x: 2, y: 2, z: 4, core: 2. Of those that a mesh axis runs over, the one named last changes fastest.
Arguments:
- query_rows: bfloat16 [16384, 1024], P('ep', 'tp'), may hold values from -6 to 6
- key_rows: bfloat16 [16384, 1024], P('ep', 'tp'), may hold values from -6 to 6
- value_rows: bfloat16 [16384, 2048], P('ep', 'tp'), may hold values from -6 to 6
- gate_rows: bfloat16 [16384, 2048], P('ep', 'tp'), may hold values from -6 to 6
- log_decay: float32 [8, 16384], P('tp', 'ep'), may hold values from -1 to 0
- out_proj: bfloat16 [2048, 2048], P('tp'), may hold values from -0.125 to 0.125
- moe_input: bfloat16 [4096, 2048], P(('ep', 'tp')), may hold values from -6 to 6
- norm_gain: float32 [2048], replicated, may hold values from 0.1 to 1.9
- routing: int32 [4096, 4], P(('ep', 'tp')), may hold values from 0 to 31, all different within a row; in each aligned block of 128 rows (0 to 127, 128 to 255, ...) at most 32 rows name the same one
- route_weight: float32 [4096, 4], P(('ep', 'tp')), may hold values from 0.2 to 1
- expert_gate: bfloat16 [32, 2048, 512], P(('ep', 'tp')), may hold values from -0.125 to 0.125
- expert_up: bfloat16 [32, 2048, 512], P(('ep', 'tp')), may hold values from -0.125 to 0.125
- expert_down: bfloat16 [32, 512, 2048], P(('ep', 'tp')), may hold values from -0.25 to 0.25
- shared_gate: bfloat16 [2048, 512], replicated, may hold values from -0.125 to 0.125
- shared_up: bfloat16 [2048, 512], replicated, may hold values from -0.125 to 0.125
- shared_down: bfloat16 [512, 2048], replicated, may hold values from -0.25 to 0.25
Outputs:
- mixer_out: bfloat16 [16384, 2048], P(('ep', 'tp'))
- moe_out: bfloat16 [4096, 2048], P(('ep', 'tp'))
Inputs may be any that keep to these rules, and one draw needn't show every extreme that they name: `routing`: within the rows of one device no expert is named more than 32 times.
All inputs are finite; a program needn't handle non-finite values.
Results may differ from a plain program's by a relative error of at most 0.019.
Values may be sent and summed in bfloat16 or wider, within the bound.
A program may use at most 128 MiB of HBM per device.

v0:
```python
import functools
import math

import jax
import jax.numpy as jnp
from jax import lax
from jax.experimental import pallas as pl
from jax.experimental.pallas import tpu as pltpu
from jax.sharding import PartitionSpec as P

DK = 128
DV = 256
BLOCK = 128
EPS = 1e-06
Z_GROUPS = 4

F32 = jnp.float32
BF16 = jnp.bfloat16
MESH = pl.DeviceIdType.MESH


def dot(a, b):
    return jnp.dot(a, b, preferred_element_type=F32)


def silu(v):
    return v / (1.0 + jnp.exp(-v))


def kernel(
    E, T, G, C,
    x_ref, gain_ref, meta_ref, cum_ref, cumc_ref, tot_ref,
    q_hbm, k_hbm, v_hbm, g_hbm, op_hbm,
    wg_hbm, wu_hbm, wd_hbm, sg_hbm, su_hbm, sd_hbm,
    mix_ref, moe_ref,
    q_v, k_v, v_v, g_v, op_v, wg_v, wu_v, wd_v,
    xz, mz, dsp, rcv, ret, dwt, shr, prcv,
    upd, sblk, lend, srcv, trcv, rs, rr, inc,
    load_sem,
    z_s, z_r, m_s, m_r, d_s, d_r, b_s, b_r, p_s, p_r, s_s, s_r, t_s, t_r, o_s, o_r, r_s, r_r,
):
    ep = lax.axis_index("ep")
    tp = lax.axis_index("tp")
    R = E // G
    Pn = R * T
    zi = ep // R
    yi = ep % R
    j = yi * T + tp
    tok, width = x_ref.shape
    n_visits = meta_ref.shape[0] // 2
    nb = cum_ref.shape[0]
    H = cum_ref.shape[1]
    nbc = nb // T
    scale = DK ** (-0.5)

    loads = [
        pltpu.make_async_copy(src, dst, load_sem.at[i])
        for i, (src, dst) in enumerate(
            ((k_hbm, k_v), (v_hbm, v_v), (op_hbm, op_v.at[0]), (sg_hbm, wg_v), (su_hbm, wu_v),
             (sd_hbm, wd_v), (q_hbm, q_v), (g_hbm, g_v), (wg_hbm.at[0], wg_v),
             (wu_hbm.at[0], wu_v), (wd_hbm.at[0], wd_v))
        )
    ]
    for c in loads[:8]:
        c.start()

    def z_peer(r):
        return (((zi + r) % G) * R + yi, tp)

    def plane_peer(d):
        p = (j + d) % Pn
        return (zi * R + p // T, p % T)

    def tp_peer(i):
        return (ep, (tp + i) % T)

    barrier = pltpu.get_barrier_semaphore()

    @pl.loop(1, Pn)
    def _(d):
        pl.semaphore_signal(barrier, inc=1, device_id=plane_peer(d), device_id_type=MESH)

    @pl.loop(1, E)
    def _(d):
        pl.semaphore_signal(barrier, inc=1, device_id=((ep + d) % E, tp), device_id_type=MESH)

    xf = x_ref[...].astype(F32)
    xz[0] = (
        xf * lax.rsqrt(jnp.mean(xf * xf, axis=-1, keepdims=True) + EPS) * gain_ref[...]
    ).astype(BF16)
    mz[0] = meta_ref[...]
    pl.semaphore_wait(barrier, Pn - 1 + E - 1)

    def rcopy(src, dst, ss, rs_, dev):
        return pltpu.make_async_remote_copy(
            src_ref=src, dst_ref=dst, send_sem=ss, recv_sem=rs_, device_id=dev, device_id_type=MESH
        )

    def z_copy(r):
        return rcopy(xz.at[0], xz.at[r], z_s.at[r], z_r.at[r], z_peer(r))

    def m_copy(r):
        return rcopy(mz.at[0], mz.at[r], m_s.at[r], m_r.at[r], z_peer(r))

    def rows(d):
        return pl.ds(pl.multiple_of(d * C, C), C)

    def d_copy(r, d):
        return rcopy(dsp.at[r, rows(d)], rcv.at[r, rows(d)], d_s.at[r, d], d_r.at[r, d],
                     plane_peer(d))

    def b_copy(r, d):
        return rcopy(rcv.at[r, rows(d)], ret.at[r, rows(d)], b_s.at[r, d], b_r.at[r, d],
                     plane_peer(Pn - d))

    def p_copy(r):
        return rcopy(dsp.at[r, 0:tok], prcv.at[r - 1], p_s.at[r], p_r.at[r], z_peer(G - r))

    def s_copy(d):
        return rcopy(lend, srcv.at[d - 1], s_s.at[d], s_r.at[d], ((ep + d) % E, tp))

    def t_copy(d):
        return rcopy(tot_ref, trcv.at[d], t_s.at[d], t_r.at[d], ((ep + d) % E, tp))

    def o_copy(i):
        return rcopy(op_v.at[0], op_v.at[i], o_s.at[i], o_r.at[i], tp_peer(i))

    def r_copy(i):
        return rcopy(rs.at[i], rr.at[i - 1], r_s.at[i], r_r.at[i], tp_peer(i))

    @pl.loop(1, G)
    def _(r):
        m_copy(r).start()
        z_copy(r).start()

    def dispatch(r):
        meta = mz[r]
        owner = lax.broadcasted_iota(jnp.int32, (Pn, tok), 0)
        owner = (zi * Pn + (owner + j) % Pn).astype(F32)
        member = jnp.zeros((Pn, tok), F32)
        weight = jnp.zeros((Pn, tok), F32)
        for v in range(n_visits):
            hit = meta[v:v + 1, :] == owner
            member += jnp.where(hit, 1.0, 0.0)
            weight += jnp.where(hit, meta[n_visits + v:n_visits + v + 1, :], 0.0)
        before = lax.broadcasted_iota(jnp.int32, (tok, tok), 0) < lax.broadcasted_iota(
            jnp.int32, (tok, tok), 1
        )
        rank = dot(member.astype(BF16), jnp.where(before, 1.0, 0.0).astype(BF16))
        rank = jnp.where(member > 0.5, rank, -1.0)
        slot = lax.broadcasted_iota(jnp.int32, (C, tok), 0).astype(F32)
        picks, wts = [], []
        for d in range(Pn):
            eq = slot == rank[d:d + 1, :]
            picks.append(jnp.where(eq, 1.0, 0.0))
            wts.append(jnp.where(eq, weight[d:d + 1, :], 0.0))
        pick = jnp.concatenate(picks, axis=0).astype(BF16)
        dwt[r] = jnp.concatenate(wts, axis=0).T.astype(BF16)
        out = dot(pick, xz[r]).astype(BF16)
        dsp[r] = out
        rcv[r, 0:C] = out[0:C]

        @pl.loop(1, Pn)
        def _(d):
            d_copy(r, d).start()

    dispatch(0)

    loads[0].wait()
    loads[1].wait()

    inc[...] = jnp.zeros_like(inc)

    @pl.loop(0, nb)
    def _(b):
        rb = pl.ds(pl.multiple_of(b * BLOCK, BLOCK), BLOCK)
        cumc = cumc_ref[b]
        crow = cum_ref[b]
        for h in range(H):
            col = cumc[:, h:h + 1]
            last = crow[h:h + 1, BLOCK - 1:BLOCK]
            u = (k_v[rb, h * DK:(h + 1) * DK].astype(F32) * (scale * jnp.exp(last - col))).astype(BF16)
            add = lax.dot_general(
                u, v_v[rb, h * DV:(h + 1) * DV], (((0,), (0,)), ((), ())),
                preferred_element_type=F32,
            )
            upd[b, h] = add
            inc[h] = inc[h] * jnp.exp(last) + add

    lend[...] = inc[...].astype(BF16)

    @pl.loop(1, E)
    def _(d):
        @pl.when(ep + d < E)
        def _():
            t_copy(d).start()
            s_copy(d).start()

    @pl.loop(1, G)
    def _(r):
        m_copy(r).wait_recv()
        z_copy(r).wait_recv()
        dispatch(r)

    loads[2].wait()

    @pl.loop(1, T)
    def _(i):
        o_copy(i).start()

    loads[3].wait()
    loads[4].wait()
    loads[5].wait()
    hid = (silu(dot(xz[0], wg_v[...])) * dot(xz[0], wu_v[...])).astype(BF16)
    shr[...] = dot(hid, wd_v[...])
    for c in loads[8:]:
        c.start()

    inc[...] = jnp.zeros_like(inc)

    @pl.loop(1, E)
    def _(i):
        d = E - i

        @pl.when(ep >= d)
        def _():
            t_copy(d).wait_recv()
            s_copy(d).wait_recv()
            for h in range(H):
                shrink = jnp.exp(trcv[d, h:h + 1, 0:1])
                inc[h] = inc[h] * shrink + srcv[d - 1, h].astype(F32)

    @pl.loop(0, nb)
    def _(b):
        crow = cum_ref[b]
        for h in range(H):
            s = inc[h]
            sblk[b, h] = s.astype(BF16)
            inc[h] = s * jnp.exp(crow[h:h + 1, BLOCK - 1:BLOCK]) + upd[b, h]

    loads[6].wait()
    loads[7].wait()
    causal = lax.broadcasted_iota(jnp.int32, (BLOCK, BLOCK), 0) >= lax.broadcasted_iota(
        jnp.int32, (BLOCK, BLOCK), 1
    )

    def retain(i):
        chunk = (tp + i) % T

        @pl.loop(0, nbc)
        def _(w):
            b = chunk * nbc + w
            rb = pl.ds(pl.multiple_of(b * BLOCK, BLOCK), BLOCK)
            ro = pl.ds(pl.multiple_of(w * BLOCK, BLOCK), BLOCK)
            cumc = cumc_ref[b]
            crow = cum_ref[b]
            for h in range(H):
                col = cumc[:, h:h + 1]
                row = crow[h:h + 1, :]
                qb = q_v[rb, h * DK:(h + 1) * DK]
                kb = k_v[rb, h * DK:(h + 1) * DK]
                vb = v_v[rb, h * DV:(h + 1) * DV]
                sc = lax.dot_general(qb, kb, (((1,), (1,)), ((), ())), preferred_element_type=F32)
                dec = jnp.exp(jnp.where(causal, col - row, 0.0))
                wt = jnp.where(causal, sc * scale * dec, 0.0).astype(BF16)
                raw = dot(wt, vb) + dot(qb, sblk[b, h]) * jnp.exp(col)
                avg = jnp.mean(raw, axis=-1, keepdims=True)
                cen = raw - avg
                var = jnp.mean(cen * cen, axis=-1, keepdims=True)
                gate = g_v[rb, h * DV:(h + 1) * DV].astype(F32)
                rs[i, ro, h * DV:(h + 1) * DV] = (
                    silu(gate) * (cen * lax.rsqrt(var + EPS))
                ).astype(BF16)

    @pl.loop(1, T)
    def _(i):
        retain(i)
        r_copy(i).start()

    retain(0)

    loads[8].wait()
    loads[9].wait()
    loads[10].wait()

    @pl.loop(0, G)
    def _(r):
        @pl.loop(1, Pn)
        def _(d):
            d_copy(r, d).wait_recv()

        rows_in = rcv[r]
        hidden = (silu(dot(rows_in, wg_v[...])) * dot(rows_in, wu_v[...])).astype(BF16)
        res = dot(hidden, wd_v[...]).astype(BF16)
        rcv[r] = res
        ret[r, 0:C] = res[0:C]

        @pl.loop(1, Pn)
        def _(d):
            b_copy(r, d).start()

    @pl.loop(1, G)
    def _(r):
        @pl.loop(1, Pn)
        def _(d):
            b_copy(r, d).wait_recv()

        @pl.loop(1, Pn)
        def _(d):
            d_copy(r, d).wait_send()

        dsp[r, 0:tok] = dot(dwt[r], ret[r]).astype(BF16)
        p_copy(r).start()

    @pl.loop(1, T)
    def _(i):
        o_copy(i).wait_recv()
        r_copy(i).wait_recv()

    n_col = 512
    @pl.loop(0, width // n_col)
    def _(n):
        cols = pl.ds(pl.multiple_of(n * n_col, n_col), n_col)
        acc = dot(rs[0], op_v[0, :, cols])
        for i in range(1, T):
            acc += dot(rr[i - 1], op_v[i, :, cols])
        mix_ref[:, cols] = acc.astype(BF16)

    @pl.loop(1, Pn)
    def _(d):
        b_copy(0, d).wait_recv()

    total = dot(dwt[0], ret[0]) + shr[...]
    for r in range(1, G):
        p_copy(r).wait_recv()
        total += prcv[r - 1].astype(F32)
    moe_ref[...] = total.astype(BF16)

    @pl.loop(1, G)
    def _(r):
        m_copy(r).wait_send()
        z_copy(r).wait_send()
        p_copy(r).wait_send()

    @pl.loop(0, G)
    def _(r):
        @pl.loop(1, Pn)
        def _(d):
            b_copy(r, d).wait_send()

    @pl.loop(1, Pn)
    def _(d):
        d_copy(0, d).wait_send()

    @pl.loop(1, E)
    def _(d):
        @pl.when(ep + d < E)
        def _():
            t_copy(d).wait_send()
            s_copy(d).wait_send()

    @pl.loop(1, T)
    def _(i):
        o_copy(i).wait_send()
        r_copy(i).wait_send()


def local(
    query_rows, key_rows, value_rows, gate_rows, log_decay, out_proj,
    moe_input, norm_gain, routing, route_weight,
    expert_gate, expert_up, expert_down, shared_gate, shared_up, shared_down,
):
    E, T = lax.axis_size("ep"), lax.axis_size("tp")
    G = math.gcd(E, Z_GROUPS)
    Pn = (E // G) * T
    n = query_rows.shape[0]
    H = query_rows.shape[1] // DK
    nb = n // BLOCK
    tok, width = moe_input.shape
    visits = routing.shape[1]
    C = 2 * tok * visits // (E * T)
    ff = expert_gate.shape[2]
    assert shared_gate.shape[1] == ff
    rows_o = n // T
    dvl = H * DV

    cum = jnp.cumsum(log_decay.reshape(H, nb, BLOCK), axis=2)
    tot = jnp.sum(cum[:, :, -1], axis=1)
    tot = jnp.broadcast_to(jnp.pad(tot, (0, -H % 8))[:, None], (H + (-H % 8), 128))
    cum_b = cum.transpose(1, 0, 2)
    cum_c = cum.transpose(1, 2, 0)
    meta = jnp.concatenate([routing.T.astype(F32), route_weight.T], axis=0)

    vm = pl.BlockSpec(memory_space=pltpu.VMEM)
    hb = pl.BlockSpec(memory_space=pl.ANY)
    V = pltpu.VMEM
    dma = pltpu.SemaphoreType.DMA
    scratch = [
        V((n, H * DK), BF16), V((n, H * DK), BF16), V((n, dvl), BF16), V((n, dvl), BF16),
        V((T,) + out_proj.shape, BF16),
        V((width, ff), BF16), V((width, ff), BF16), V((ff, width), BF16),
        V((G, tok, width), BF16), V((G, 2 * visits, tok), F32),
        V((G, Pn * C, width), BF16), V((G, Pn * C, width), BF16), V((G, Pn * C, width), BF16),
        V((G, tok, Pn * C), BF16), V((tok, width), F32), V((G - 1, tok, width), BF16),
        V((nb, H, DK, DV), F32), V((nb, H, DK, DV), BF16), V((H, DK, DV), BF16),
        V((E - 1, H, DK, DV), BF16), V((E,) + tot.shape, F32),
        V((T, rows_o, dvl), BF16), V((T - 1, rows_o, dvl), BF16), V((H, DK, DV), F32),
        dma((11,)),
        dma((G,)), dma((G,)), dma((G,)), dma((G,)),
        dma((G, Pn)), dma((G, Pn)), dma((G, Pn)), dma((G, Pn)),
        dma((G,)), dma((G,)),
        dma((E,)), dma((E,)), dma((E,)), dma((E,)),
        dma((T,)), dma((T,)), dma((T,)), dma((T,)),
    ]
    return pl.pallas_call(
        functools.partial(kernel, E, T, G, C),
        out_shape=(
            jax.ShapeDtypeStruct((rows_o, width), BF16),
            jax.ShapeDtypeStruct((tok, width), BF16),
        ),
        in_specs=[vm] * 6 + [hb] * 11,
        out_specs=(vm, vm),
        scratch_shapes=scratch,
        compiler_params=pltpu.CompilerParams(
            collective_id=0, has_side_effects=True, vmem_limit_bytes=67043328
        ),
        name="fused",
    )(
        moe_input, norm_gain[None, :], meta, cum_b, cum_c, tot,
        query_rows, key_rows, value_rows, gate_rows, out_proj,
        expert_gate, expert_up, expert_down, shared_gate, shared_up, shared_down,
    )


def solution(mesh):
    both = P(("ep", "tp"), None)
    in_specs = (
        P("ep", "tp"), P("ep", "tp"), P("ep", "tp"), P("ep", "tp"), P("tp", "ep"), P("tp", None),
        both, P(), both, both,
        P(("ep", "tp"), None, None), P(("ep", "tp"), None, None), P(("ep", "tp"), None, None),
        P(), P(), P(),
    )
    return jax.shard_map(
        local, mesh=mesh, in_specs=in_specs, out_specs=(both, both), check_vma=False
    )
```

profile of v0, /device:TPU:2, one launch (start us, length us, event | category | flops | bytes accessed | tf_op | source)
XLA Modules:
  0.0 274.5 jit_solution(2051693459938543831)
XLA Ops:
  0.6 0.7 convert_bitcast_fusion
  1.3 1.3 pad_maximum_fusion.meta_ref
  2.6 0.7 copy.23
  3.3 0.6 reduce_window_sum.11
  3.9 0.2 slice_reduce_fusion
  4.1 0.7 broadcast_in_dim.10.tot_ref
  4.7 0.6 copy.24
  5.3 1.3 copy.19
  6.7 263.8 %fused.1 = (bf16[512,2048]{1,0:T(8,128)(2,1)}, bf16[128,2048]{1,0:T(8,128)(2,1)}) custom-call(bf16[128,2048]{1,0:T(8,128)(2,1)} %x_ref.1, f32[1,2048]{1,0:T(1,128)} %bitcast.16, f32[8,128]{1,0:T(8,128)} %pad_maximum_fusion.meta_ref, f32[16,2,128]{2,1,0:T(2,128)} %bitcast.14, f32[16,128,2]{2,1,0:T(8,128)} %bitcast.12, f32[8,128]{1,0:T(8,128)} %broadcast_in_dim.10.tot_ref, ...), custom_call_target="tpu_custom_call" | custom-call | tf_op jit(solution)/shard_map/fused/pallas_call | solution.py:415
  270.5 0.0 copy-start
  270.5 3.2 %copy.27 = bf16[512,2048]{1,0:T(8,128)(2,1)} copy(bf16[512,2048]{1,0:T(8,128)(2,1)} %get-tuple-element.4) | data formatting | bytes 4194304
  273.7 0.0 copy-done
  273.7 0.8 copy.28
  (1 shorter events, 0.0 us)
Async XLA Ops:
  270.5 3.2 %copy-start = (bf16[128,2048]{1,0:T(8,128)(2,1)S(1)}, bf16[128,2048]{1,0:T(8,128)(2,1)}, u32[]{:S(2)}) copy-start(bf16[128,2048]{1,0:T(8,128)(2,1)} %get-tuple-element.5) | copy-start | bytes 1572868
where the time goes:
time: 277 us; the launch traced here: 275 us
  Pallas kernels  264 us (95%)
  local copies, waits for them, and re-layouts  7.37 us (3%)
    pallas_call x1, Pallas kernels, local(): pl.pallas_call(functools.partial(kernel, E, T, G, C), out_shape=(jax.Shap...  264 us

commit v1 on v0

--- a/solution.py
+++ b/solution.py
@@ -37,7 +37,8 @@
     xz, mz, dsp, rcv, ret, dwt, shr, prcv,
     upd, sblk, lend, srcv, trcv, rs, rr, inc,
     load_sem,
-    z_s, z_r, m_s, m_r, d_s, d_r, b_s, b_r, p_s, p_r, s_s, s_r, t_s, t_r, o_s, o_r, r_s, r_r,
+    z_s, z_r, m_s, m_r, d_s, d_r, b_s, b_r, p_s, p_r, s_s, s_r, t_s, t_r,
+    o1_s, o1_r, o2_s, o2_r, o3_s, o3_r, r_s, r_r,
 ):
     ep = lax.axis_index("ep")
     tp = lax.axis_index("tp")
@@ -51,12 +52,16 @@
     nb = cum_ref.shape[0]
     H = cum_ref.shape[1]
     nbc = nb // T
+    B = math.gcd(T, 2)
+    A = T // B
+    ta, tb = tp // B, tp % B
+    piece = op_v.shape[1] // R
     scale = DK ** (-0.5)
 
     loads = [
         pltpu.make_async_copy(src, dst, load_sem.at[i])
         for i, (src, dst) in enumerate(
-            ((k_hbm, k_v), (v_hbm, v_v), (op_hbm, op_v.at[0]), (sg_hbm, wg_v), (su_hbm, wu_v),
+            ((k_hbm, k_v), (v_hbm, v_v), (op_hbm, op_v.at[tp]), (sg_hbm, wg_v), (su_hbm, wu_v),
              (sd_hbm, wd_v), (q_hbm, q_v), (g_hbm, g_v), (wg_hbm.at[0], wg_v),
              (wu_hbm.at[0], wu_v), (wd_hbm.at[0], wd_v))
         )
@@ -64,8 +69,8 @@
     for c in loads[:8]:
         c.start()
 
-    def z_peer(r):
-        return (((zi + r) % G) * R + yi, tp)
+    def z_place(g):
+        return (g * R + yi, tp)
 
     def plane_peer(d):
         p = (j + d) % Pn
@@ -85,10 +90,10 @@
         pl.semaphore_signal(barrier, inc=1, device_id=((ep + d) % E, tp), device_id_type=MESH)
 
     xf = x_ref[...].astype(F32)
-    xz[0] = (
+    xz[zi] = (
         xf * lax.rsqrt(jnp.mean(xf * xf, axis=-1, keepdims=True) + EPS) * gain_ref[...]
     ).astype(BF16)
-    mz[0] = meta_ref[...]
+    mz[zi] = meta_ref[...]
     pl.semaphore_wait(barrier, Pn - 1 + E - 1)
 
     def rcopy(src, dst, ss, rs_, dev):
@@ -96,11 +101,23 @@
             src_ref=src, dst_ref=dst, send_sem=ss, recv_sem=rs_, device_id=dev, device_id_type=MESH
         )
 
-    def z_copy(r):
-        return rcopy(xz.at[0], xz.at[r], z_s.at[r], z_r.at[r], z_peer(r))
-
-    def m_copy(r):
-        return rcopy(mz.at[0], mz.at[r], m_s.at[r], m_r.at[r], z_peer(r))
+    def z_copy(g, way):
+        to = (zi - 1, zi + 1)[way]
+        return rcopy(xz.at[g], xz.at[g], z_s.at[way, g], z_r.at[g], z_place(to))
+
+    def m_copy(g, way):
+        to = (zi - 1, zi + 1)[way]
+        return rcopy(mz.at[g], mz.at[g], m_s.at[way, g], m_r.at[g], z_place(to))
+
+    def z_sends(g, way):
+        if way:
+            return (g <= zi) & (zi + 1 < G)
+        return (g >= zi) & (zi > 0)
+
+    def group_at(i):
+        dist = (i + 1) // 2
+        g = zi + jnp.where(i % 2 == 1, -dist, dist)
+        return g, (g >= 0) & (g < G)
 
     def rows(d):
         return pl.ds(pl.multiple_of(d * C, C), C)
@@ -113,8 +130,11 @@
         return rcopy(rcv.at[r, rows(d)], ret.at[r, rows(d)], b_s.at[r, d], b_r.at[r, d],
                      plane_peer(Pn - d))
 
-    def p_copy(r):
-        return rcopy(dsp.at[r, 0:tok], prcv.at[r - 1], p_s.at[r], p_r.at[r], z_peer(G - r))
+    def p_copy(g):
+        return rcopy(dsp.at[g, 0:tok], prcv.at[zi], p_s.at[g], p_r.at[zi], z_place(g))
+
+    def p_arrival(g):
+        return rcopy(dsp.at[g, 0:tok], prcv.at[g], p_s.at[g], p_r.at[g], z_place(g))
 
     def s_copy(d):
         return rcopy(lend, srcv.at[d - 1], s_s.at[d], s_r.at[d], ((ep + d) % E, tp))
@@ -122,16 +142,32 @@
     def t_copy(d):
         return rcopy(tot_ref, trcv.at[d], t_s.at[d], t_r.at[d], ((ep + d) % E, tp))
 
-    def o_copy(i):
-        return rcopy(op_v.at[0], op_v.at[i], o_s.at[i], o_r.at[i], tp_peer(i))
+    def shard(da, db=0):
+        return ((ta + A - da) % A) * B + (tb + B - db) % B
+
+    def part(y):
+        return pl.ds(pl.multiple_of(y * piece, piece), piece)
+
+    def o1_copy(da, src):
+        at = op_v.at[src, part(yi)]
+        return rcopy(at, at, o1_s.at[da], o1_r.at[da], (ep, ((ta + da) % A) * B + tb))
+
+    def o2_copy(da, dy, y):
+        at = op_v.at[shard(da), part(y)]
+        return rcopy(at, at, o2_s.at[da, dy], o2_r.at[da, dy], (zi * R + (yi + dy) % R, tp))
+
+    def o3_copy(da, db, src):
+        at = op_v.at[src]
+        return rcopy(at, at, o3_s.at[da, db], o3_r.at[da, db], (ep, ta * B + (tb + db) % B))
 
     def r_copy(i):
         return rcopy(rs.at[i], rr.at[i - 1], r_s.at[i], r_r.at[i], tp_peer(i))
 
-    @pl.loop(1, G)
-    def _(r):
-        m_copy(r).start()
-        z_copy(r).start()
+    for way in (0, 1):
+        @pl.when(z_sends(zi, way))
+        def _():
+            m_copy(zi, way).start()
+            z_copy(zi, way).start()
 
     def dispatch(r):
         meta = mz[r]
@@ -164,7 +200,10 @@
         def _(d):
             d_copy(r, d).start()
 
-    dispatch(0)
+    dispatch(zi)
+    loads[2].wait()
+    for da in range(1, A):
+        o1_copy(da, tp).start()
 
     loads[0].wait()
     loads[1].wait()
@@ -196,22 +235,32 @@
             t_copy(d).start()
             s_copy(d).start()
 
-    @pl.loop(1, G)
-    def _(r):
-        m_copy(r).wait_recv()
-        z_copy(r).wait_recv()
-        dispatch(r)
-
-    loads[2].wait()
-
-    @pl.loop(1, T)
-    def _(i):
-        o_copy(i).start()
+    @pl.loop(1, 2 * G - 1)
+    def _(i):
+        g, there = group_at(i)
+
+        @pl.when(there)
+        def _():
+            m_copy(g, 0).wait_recv()
+            z_copy(g, 0).wait_recv()
+            for way in (0, 1):
+                @pl.when(z_sends(g, way))
+                def _():
+                    m_copy(g, way).start()
+                    z_copy(g, way).start()
+            dispatch(g)
+
+    for da in range(1, A):
+        o1_copy(da, shard(da)).wait_recv()
+        for dy in range(1, R):
+            o2_copy(da, dy, yi).start()
+    for db in range(1, B):
+        o3_copy(0, db, tp).start()
 
     loads[3].wait()
     loads[4].wait()
     loads[5].wait()
-    hid = (silu(dot(xz[0], wg_v[...])) * dot(xz[0], wu_v[...])).astype(BF16)
+    hid = (silu(dot(xz[zi], wg_v[...])) * dot(xz[zi], wu_v[...])).astype(BF16)
     shr[...] = dot(hid, wd_v[...])
     for c in loads[8:]:
         c.start()
@@ -275,7 +324,6 @@
     @pl.loop(1, T)
     def _(i):
         retain(i)
-        r_copy(i).start()
 
     retain(0)
 
@@ -283,8 +331,7 @@
     loads[9].wait()
     loads[10].wait()
 
-    @pl.loop(0, G)
-    def _(r):
+    def serve(r):
         @pl.loop(1, Pn)
         def _(d):
             d_copy(r, d).wait_recv()
@@ -299,8 +346,25 @@
         def _(d):
             b_copy(r, d).start()
 
-    @pl.loop(1, G)
-    def _(r):
+    @pl.loop(0, 2 * G - 1)
+    def _(i):
+        g, there = group_at(i)
+
+        @pl.when(there)
+        def _():
+            serve(g)
+
+    @pl.loop(1, T)
+    def _(i):
+        r_copy(i).start()
+
+    for da in range(1, A):
+        for dy in range(1, R):
+            o2_copy(da, dy, (yi + R - dy) % R).wait_recv()
+        for db in range(1, B):
+            o3_copy(da, db, shard(da)).start()
+
+    def combine(r):
         @pl.loop(1, Pn)
         def _(d):
             b_copy(r, d).wait_recv()
@@ -312,35 +376,56 @@
         dsp[r, 0:tok] = dot(dwt[r], ret[r]).astype(BF16)
         p_copy(r).start()
 
+    @pl.loop(1, 2 * G - 1)
+    def _(i):
+        g, there = group_at(i)
+
+        @pl.when(there)
+        def _():
+            combine(g)
+
+    for da in range(A):
+        for db in range(1, B):
+            o3_copy(da, db, shard(da, db)).wait_recv()
+
     @pl.loop(1, T)
     def _(i):
-        o_copy(i).wait_recv()
         r_copy(i).wait_recv()
 
     n_col = 512
     @pl.loop(0, width // n_col)
     def _(n):
         cols = pl.ds(pl.multiple_of(n * n_col, n_col), n_col)
-        acc = dot(rs[0], op_v[0, :, cols])
+        acc = dot(rs[0], op_v[tp, :, cols])
         for i in range(1, T):
-            acc += dot(rr[i - 1], op_v[i, :, cols])
+            acc += dot(rr[i - 1], op_v[(tp + T - i) % T, :, cols])
         mix_ref[:, cols] = acc.astype(BF16)
 
     @pl.loop(1, Pn)
     def _(d):
-        b_copy(0, d).wait_recv()
-
-    total = dot(dwt[0], ret[0]) + shr[...]
-    for r in range(1, G):
-        p_copy(r).wait_recv()
-        total += prcv[r - 1].astype(F32)
-    moe_ref[...] = total.astype(BF16)
+        b_copy(zi, d).wait_recv()
+
+    shr[...] += dot(dwt[zi], ret[zi])
 
     @pl.loop(1, G)
-    def _(r):
-        m_copy(r).wait_send()
-        z_copy(r).wait_send()
-        p_copy(r).wait_send()
+    def _(i):
+        g = (zi + i) % G
+        p_arrival(g).wait_recv()
+        shr[...] += prcv[g].astype(F32)
+
+    moe_ref[...] = shr[...].astype(BF16)
+
+    @pl.loop(0, G)
+    def _(g):
+        for way in (0, 1):
+            @pl.when(z_sends(g, way))
+            def _():
+                m_copy(g, way).wait_send()
+                z_copy(g, way).wait_send()
+
+        @pl.when(g != zi)
+        def _():
+            p_copy(g).wait_send()
 
     @pl.loop(0, G)
     def _(r):
@@ -350,7 +435,7 @@
 
     @pl.loop(1, Pn)
     def _(d):
-        d_copy(0, d).wait_send()
+        d_copy(zi, d).wait_send()
 
     @pl.loop(1, E)
     def _(d):
@@ -361,8 +446,15 @@
 
     @pl.loop(1, T)
     def _(i):
-        o_copy(i).wait_send()
         r_copy(i).wait_send()
+
+    for da in range(A):
+        if da:
+            o1_copy(da, tp).wait_send()
+            for dy in range(1, R):
+                o2_copy(da, dy, yi).wait_send()
+        for db in range(1, B):
+            o3_copy(da, db, shard(da)).wait_send()
 
 
 def local(
@@ -401,16 +493,17 @@
         V((width, ff), BF16), V((width, ff), BF16), V((ff, width), BF16),
         V((G, tok, width), BF16), V((G, 2 * visits, tok), F32),
         V((G, Pn * C, width), BF16), V((G, Pn * C, width), BF16), V((G, Pn * C, width), BF16),
-        V((G, tok, Pn * C), BF16), V((tok, width), F32), V((G - 1, tok, width), BF16),
+        V((G, tok, Pn * C), BF16), V((tok, width), F32), V((G, tok, width), BF16),
         V((nb, H, DK, DV), F32), V((nb, H, DK, DV), BF16), V((H, DK, DV), BF16),
         V((E - 1, H, DK, DV), BF16), V((E,) + tot.shape, F32),
         V((T, rows_o, dvl), BF16), V((T - 1, rows_o, dvl), BF16), V((H, DK, DV), F32),
         dma((11,)),
-        dma((G,)), dma((G,)), dma((G,)), dma((G,)),
+        dma((2, G)), dma((G,)), dma((2, G)), dma((G,)),
         dma((G, Pn)), dma((G, Pn)), dma((G, Pn)), dma((G, Pn)),
         dma((G,)), dma((G,)),
         dma((E,)), dma((E,)), dma((E,)), dma((E,)),
-        dma((T,)), dma((T,)), dma((T,)), dma((T,)),
+        dma((T,)), dma((T,)), dma((T, E)), dma((T, E)), dma((T, T)), dma((T, T)),
+        dma((T,)), dma((T,)),
     ]
     return pl.pallas_call(
         functools.partial(kernel, E, T, G, C),

time: 277 us -> 190 us (0.69)
  Pallas kernels: 264 us -> 179 us
    pallas_call x1, Pallas kernels: 264 us -> 179 us  [local(): pl.pallas_call(functools.partial(kernel, E, T, G, C), out_shape=(jax.Shap...]
where the time goes in v1:
time: 190 us; the launch traced here: 189 us
  Pallas kernels  179 us (94%)
  local copies, waits for them, and re-layouts  7.37 us (4%)
  other arithmetic  2.7 us (1%)
    pallas_call x1, Pallas kernels, local(): pl.pallas_call(functools.partial(kernel, E, T, G, C), out_shape=(jax.Shap...  179 us
    unnamed x5, local copies, waits for them, and re-layouts  4.73 us

profile of v1, /device:TPU:2, one launch (start us, length us, event | category | flops | bytes accessed | tf_op | source)
XLA Modules:
  0.0 189.2 jit_solution(9909629746390916582)
XLA Ops:
  0.6 0.7 convert_bitcast_fusion
  1.3 1.3 pad_maximum_fusion.meta_ref
  2.6 0.7 copy.23
  3.3 0.6 reduce_window_sum.11
  3.9 0.2 slice_reduce_fusion
  4.1 0.7 broadcast_in_dim.10.tot_ref
  4.7 0.6 copy.24
  5.3 1.3 copy.19
  6.7 178.5 %fused.1 = (bf16[512,2048]{1,0:T(8,128)(2,1)}, bf16[128,2048]{1,0:T(8,128)(2,1)}) custom-call(bf16[128,2048]{1,0:T(8,128)(2,1)} %x_ref.1, f32[1,2048]{1,0:T(1,128)} %bitcast.16, f32[8,128]{1,0:T(8,128)} %pad_maximum_fusion.meta_ref, f32[16,2,128]{2,1,0:T(2,128)} %bitcast.14, f32[16,128,2]{2,1,0:T(8,128)} %bitcast.12, f32[8,128]{1,0:T(8,128)} %broadcast_in_dim.10.tot_ref, ...), custom_call_target="tpu_custom_call" | custom-call | tf_op jit(solution)/shard_map/fused/pallas_call | solution.py:508
  185.2 0.0 copy-start
  185.2 3.2 %copy.27 = bf16[512,2048]{1,0:T(8,128)(2,1)} copy(bf16[512,2048]{1,0:T(8,128)(2,1)} %get-tuple-element.4) | data formatting | bytes 4194304
  188.4 0.0 copy-done
  188.4 0.8 copy.28
  (1 shorter events, 0.0 us)
Async XLA Ops:
  185.2 3.2 %copy-start = (bf16[128,2048]{1,0:T(8,128)(2,1)S(1)}, bf16[128,2048]{1,0:T(8,128)(2,1)}, u32[]{:S(2)}) copy-start(bf16[128,2048]{1,0:T(8,128)(2,1)} %get-tuple-element.5) | copy-start | bytes 1572868

commit v2 on v1

--- a/solution.py
+++ b/solution.py
@@ -201,9 +201,6 @@
             d_copy(r, d).start()
 
     dispatch(zi)
-    loads[2].wait()
-    for da in range(1, A):
-        o1_copy(da, tp).start()
 
     loads[0].wait()
     loads[1].wait()
@@ -228,13 +225,32 @@
 
     lend[...] = inc[...].astype(BF16)
 
-    @pl.loop(1, E)
-    def _(d):
-        @pl.when(ep + d < E)
-        def _():
-            t_copy(d).start()
-            s_copy(d).start()
-
+    loads[3].wait()
+    loads[4].wait()
+    loads[5].wait()
+    hid = (silu(dot(xz[zi], wg_v[...])) * dot(xz[zi], wu_v[...])).astype(BF16)
+    shr[...] = dot(hid, wd_v[...])
+    for c in loads[8:]:
+        c.start()
+
+    def serve(r):
+        @pl.loop(1, Pn)
+        def _(d):
+            d_copy(r, d).wait_recv()
+
+        rows_in = rcv[r]
+        hidden = (silu(dot(rows_in, wg_v[...])) * dot(rows_in, wu_v[...])).astype(BF16)
+        res = dot(hidden, wd_v[...]).astype(BF16)
+        rcv[r] = res
+        ret[r, 0:C] = res[0:C]
+
+        @pl.loop(1, Pn)
+        def _(d):
+            b_copy(r, d).start()
+
+    loads[8].wait()
+    loads[9].wait()
+    loads[10].wait()
     @pl.loop(1, 2 * G - 1)
     def _(i):
         g, there = group_at(i)
@@ -250,20 +266,28 @@
                     z_copy(g, way).start()
             dispatch(g)
 
+        behind, known = group_at(i - 2)
+
+        @pl.when(known & (i >= 2))
+        def _():
+            serve(behind)
+
+    @pl.loop(1, E)
+    def _(d):
+        @pl.when(ep + d < E)
+        def _():
+            t_copy(d).start()
+            s_copy(d).start()
+
+    loads[2].wait()
     for da in range(1, A):
-        o1_copy(da, shard(da)).wait_recv()
-        for dy in range(1, R):
-            o2_copy(da, dy, yi).start()
-    for db in range(1, B):
-        o3_copy(0, db, tp).start()
-
-    loads[3].wait()
-    loads[4].wait()
-    loads[5].wait()
-    hid = (silu(dot(xz[zi], wg_v[...])) * dot(xz[zi], wu_v[...])).astype(BF16)
-    shr[...] = dot(hid, wd_v[...])
-    for c in loads[8:]:
-        c.start()
+        o1_copy(da, tp).start()
+    for i in (2 * G - 3, 2 * G - 2):
+        g, there = group_at(jnp.int32(i))
+
+        @pl.when(there)
+        def _():
+            serve(g)
 
     inc[...] = jnp.zeros_like(inc)
 
@@ -327,62 +351,42 @@
 
     retain(0)
 
-    loads[8].wait()
-    loads[9].wait()
-    loads[10].wait()
-
-    def serve(r):
+    @pl.loop(1, T)
+    def _(i):
+        r_copy(i).start()
+
+    for da in range(1, A):
+        o1_copy(da, shard(da)).wait_recv()
+        for dy in range(1, R):
+            o2_copy(da, dy, yi).start()
+    for db in range(1, B):
+        o3_copy(0, db, tp).start()
+
+    def combine(r):
         @pl.loop(1, Pn)
         def _(d):
-            d_copy(r, d).wait_recv()
-
-        rows_in = rcv[r]
-        hidden = (silu(dot(rows_in, wg_v[...])) * dot(rows_in, wu_v[...])).astype(BF16)
-        res = dot(hidden, wd_v[...]).astype(BF16)
-        rcv[r] = res
-        ret[r, 0:C] = res[0:C]
+            b_copy(r, d).wait_recv()
 
         @pl.loop(1, Pn)
         def _(d):
-            b_copy(r, d).start()
-
-    @pl.loop(0, 2 * G - 1)
+            d_copy(r, d).wait_send()
+
+        dsp[r, 0:tok] = dot(dwt[r], ret[r]).astype(BF16)
+        p_copy(r).start()
+
+    @pl.loop(1, 2 * G - 1)
     def _(i):
         g, there = group_at(i)
 
         @pl.when(there)
         def _():
-            serve(g)
-
-    @pl.loop(1, T)
-    def _(i):
-        r_copy(i).start()
+            combine(g)
 
     for da in range(1, A):
         for dy in range(1, R):
             o2_copy(da, dy, (yi + R - dy) % R).wait_recv()
         for db in range(1, B):
             o3_copy(da, db, shard(da)).start()
-
-    def combine(r):
-        @pl.loop(1, Pn)
-        def _(d):
-            b_copy(r, d).wait_recv()
-
-        @pl.loop(1, Pn)
-        def _(d):
-            d_copy(r, d).wait_send()
-
-        dsp[r, 0:tok] = dot(dwt[r], ret[r]).astype(BF16)
-        p_copy(r).start()
-
-    @pl.loop(1, 2 * G - 1)
-    def _(i):
-        g, there = group_at(i)
-
-        @pl.when(there)
-        def _():
-            combine(g)
 
     for da in range(A):
         for db in range(1, B):

time: 190 us -> 185 us (0.974)
  Pallas kernels: 179 us -> 174 us
    pallas_call x1, Pallas kernels: 179 us -> 174 us  [local(): pl.pallas_call(functools.partial(kernel, E, T, G, C), out_shape=(jax.Shap...]
where the time goes in v2:
time: 185 us
  Pallas kernels  174 us (94%)
  local copies, waits for them, and re-layouts  7.37 us (4%)
  other arithmetic  2.7 us (1%)
    pallas_call x1, Pallas kernels, local(): pl.pallas_call(functools.partial(kernel, E, T, G, C), out_shape=(jax.Shap...  174 us
    unnamed x5, local copies, waits for them, and re-layouts  4.73 us

profile of v2, /device:TPU:2, one launch (start us, length us, event | category | flops | bytes accessed | tf_op | source)
XLA Modules:
  0.0 184.6 jit_solution(15544839358548194779)
XLA Ops:
  0.6 0.7 convert_bitcast_fusion
  1.3 1.3 pad_maximum_fusion.meta_ref
  2.6 0.7 copy.23
  3.3 0.6 reduce_window_sum.11
  3.9 0.2 slice_reduce_fusion
  4.1 0.7 broadcast_in_dim.10.tot_ref
  4.7 0.6 copy.24
  5.3 1.3 copy.19
  6.7 173.9 %fused.1 = (bf16[512,2048]{1,0:T(8,128)(2,1)}, bf16[128,2048]{1,0:T(8,128)(2,1)}) custom-call(bf16[128,2048]{1,0:T(8,128)(2,1)} %x_ref.1, f32[1,2048]{1,0:T(1,128)} %bitcast.16, f32[8,128]{1,0:T(8,128)} %pad_maximum_fusion.meta_ref, f32[16,2,128]{2,1,0:T(2,128)} %bitcast.14, f32[16,128,2]{2,1,0:T(8,128)} %bitcast.12, f32[8,128]{1,0:T(8,128)} %broadcast_in_dim.10.tot_ref, ...), custom_call_target="tpu_custom_call" | custom-call | tf_op jit(solution)/shard_map/fused/pallas_call | solution.py:512
  180.6 0.0 copy-start
  180.6 3.2 %copy.27 = bf16[512,2048]{1,0:T(8,128)(2,1)} copy(bf16[512,2048]{1,0:T(8,128)(2,1)} %get-tuple-element.4) | data formatting | bytes 4194304
  183.8 0.0 copy-done
  183.8 0.8 copy.28
  (1 shorter events, 0.0 us)
Async XLA Ops:
  180.6 3.2 %copy-start = (bf16[128,2048]{1,0:T(8,128)(2,1)S(1)}, bf16[128,2048]{1,0:T(8,128)(2,1)}, u32[]{:S(2)}) copy-start(bf16[128,2048]{1,0:T(8,128)(2,1)} %get-tuple-element.5) | copy-start | bytes 1572868

commit v3 on v2

--- a/solution.py
+++ b/solution.py
@@ -266,18 +266,20 @@
                     z_copy(g, way).start()
             dispatch(g)
 
+        @pl.when(i == G - 1)
+        def _():
+            @pl.loop(1, E)
+            def _(d):
+                @pl.when(ep + d < E)
+                def _():
+                    t_copy(d).start()
+                    s_copy(d).start()
+
         behind, known = group_at(i - 2)
 
         @pl.when(known & (i >= 2))
         def _():
             serve(behind)
-
-    @pl.loop(1, E)
-    def _(d):
-        @pl.when(ep + d < E)
-        def _():
-            t_copy(d).start()
-            s_copy(d).start()
 
     loads[2].wait()
     for da in range(1, A):
@@ -355,32 +357,32 @@
     def _(i):
         r_copy(i).start()
 
+    def combine(r):
+        @pl.loop(1, Pn)
+        def _(d):
+            b_copy(r, d).wait_recv()
+
+        @pl.loop(1, Pn)
+        def _(d):
+            d_copy(r, d).wait_send()
+
+        dsp[r, 0:tok] = dot(dwt[r], ret[r]).astype(BF16)
+        p_copy(r).start()
+
+    @pl.loop(1, 2 * G - 1)
+    def _(i):
+        g, there = group_at(i)
+
+        @pl.when(there)
+        def _():
+            combine(g)
+
     for da in range(1, A):
         o1_copy(da, shard(da)).wait_recv()
         for dy in range(1, R):
             o2_copy(da, dy, yi).start()
     for db in range(1, B):
         o3_copy(0, db, tp).start()
-
-    def combine(r):
-        @pl.loop(1, Pn)
-        def _(d):
-            b_copy(r, d).wait_recv()
-
-        @pl.loop(1, Pn)
-        def _(d):
-            d_copy(r, d).wait_send()
-
-        dsp[r, 0:tok] = dot(dwt[r], ret[r]).astype(BF16)
-        p_copy(r).start()
-
-    @pl.loop(1, 2 * G - 1)
-    def _(i):
-        g, there = group_at(i)
-
-        @pl.when(there)
-        def _():
-            combine(g)
 
     for da in range(1, A):
         for dy in range(1, R):

time: 185 us -> 174 us (0.941)
  the two profiles are of different devices: /device:TPU:2 before, /device:TPU:25 now
where the time goes in v3:
time: 174 us; the launch traced here: 173 us
  Pallas kernels  163 us (94%)
  local copies, waits for them, and re-layouts  7.37 us (4%)
  other arithmetic  2.7 us (2%)
    pallas_call x1, Pallas kernels, local(): pl.pallas_call(functools.partial(kernel, E, T, G, C), out_shape=(jax.Shap...  163 us
    unnamed x5, local copies, waits for them, and re-layouts  4.73 us

profile of v3, /device:TPU:25, one launch (start us, length us, event | category | flops | bytes accessed | tf_op | source)
XLA Modules:
  0.0 173.3 jit_solution(3827343627730708154)
XLA Ops:
  0.6 0.7 convert_bitcast_fusion
  1.3 1.3 pad_maximum_fusion.meta_ref
  2.6 0.7 copy.23
  3.3 0.6 reduce_window_sum.11
  3.9 0.2 slice_reduce_fusion
  4.1 0.7 broadcast_in_dim.10.tot_ref
  4.7 0.6 copy.24
  5.3 1.3 copy.19
  6.7 162.6 %fused.1 = (bf16[512,2048]{1,0:T(8,128)(2,1)}, bf16[128,2048]{1,0:T(8,128)(2,1)}) custom-call(bf16[128,2048]{1,0:T(8,128)(2,1)} %x_ref.1, f32[1,2048]{1,0:T(1,128)} %bitcast.16, f32[8,128]{1,0:T(8,128)} %pad_maximum_fusion.meta_ref, f32[16,2,128]{2,1,0:T(2,128)} %bitcast.14, f32[16,128,2]{2,1,0:T(8,128)} %bitcast.12, f32[8,128]{1,0:T(8,128)} %broadcast_in_dim.10.tot_ref, ...), custom_call_target="tpu_custom_call" | custom-call | tf_op jit(solution)/shard_map/fused/pallas_call | solution.py:514
  169.3 0.0 copy-start
  169.3 3.2 %copy.27 = bf16[512,2048]{1,0:T(8,128)(2,1)} copy(bf16[512,2048]{1,0:T(8,128)(2,1)} %get-tuple-element.4) | data formatting | bytes 4194304
  172.5 0.0 copy-done
  172.5 0.8 copy.28
  (1 shorter events, 0.0 us)
Async XLA Ops:
  169.3 3.2 %copy-start = (bf16[128,2048]{1,0:T(8,128)(2,1)S(1)}, bf16[128,2048]{1,0:T(8,128)(2,1)}, u32[]{:S(2)}) copy-start(bf16[128,2048]{1,0:T(8,128)(2,1)} %get-tuple-element.5) | copy-start | bytes 1572868
